TPU v7x, 32 devices: a whole 2x2x4 slice. The times are simulated.
32 devices in a mesh: sp: 8 (over z, x), tp: 4 (over y, core).
Axes of the slice: x: 2, y: 2, z: 4, core: 2. Of those that a mesh axis runs over, the one named last changes fastest.
Arguments:
- tokens: bfloat16 [1024, 2048], P(('sp', 'tp')), may hold values from -6 to 6
- input_norm_gain: float32 [2048], replicated, may hold values from 0.1 to 1.9
- convolution_value_weight: bfloat16 [2048, 1024], P('sp', 'tp'), may hold values from -0.125 to 0.125
- convolution_gate_weight: bfloat16 [2048, 1024], P('sp', 'tp'), may hold values from -0.125 to 0.125
- depthwise_filter_taps: float32 [31, 1024], P(None, 'tp'), may hold values from -4 to 4
- channel_norm_gain: float32 [1024], P('tp'), may hold values from 0.1 to 1.9
- channel_norm_bias: float32 [1024], P('tp'), may hold values from -3 to 3
- query_projection_weight: bfloat16 [2048, 1024], P('sp', 'tp'), may hold values from -0.125 to 0.125
- forget_gate_weight: bfloat16 [2048, 1024], P('sp', 'tp'), may hold values from -0.125 to 0.125
- recurrence_value_weight: bfloat16 [2048, 1024], P('sp', 'tp'), may hold values from -0.125 to 0.125
- output_gate_weight: bfloat16 [2048, 1024], P('sp', 'tp'), may hold values from -0.125 to 0.125
- forget_floor_margin: float32 [1024], P('tp'), may hold values from 9.765625e-05 to 0.1
- decay_jump_terms: float32 [8, 1024], P('tp', 'sp'), may hold values from -0.7 to 0
- head_norm_gain: float32 [1024], P('tp'), may hold values from 0.1 to 1.9
- convolution_output_weight: bfloat16 [1024, 2048], P('tp', 'sp'), may hold values from -0.125 to 0.125
- recurrence_output_weight: bfloat16 [1024, 2048], P('tp', 'sp'), may hold values from -0.125 to 0.125
Outputs:
- mixed: bfloat16 [1024, 2048], P(('sp', 'tp'))
All inputs are finite; a program needn't handle non-finite values.
Results may differ from a plain program's by a relative error of at most 0.015.
Values may be sent and summed in bfloat16 or wider, within the bound.
A program may use at most 64 MiB of HBM per device.

v0:
```python
import jax
import jax.numpy as jnp
from jax import lax
from jax.sharding import PartitionSpec as P

CONV_CH = 1024
HG_DK = 128
HG_DV = 128
HG_BLOCK = 64
norm_eps = 1e-06
layer_eps = 1e-05
highest_precision = lax.Precision.HIGHEST


def passed_along(value, axis, steps):
    count = lax.axis_size(axis)
    initial, last = (max(0, -steps), min(count, count - steps))
    return lax.ppermute(value, axis, [(source, source + steps) for source in range(initial, last)])


def prefix(x, axis, combine, identity):
    size, mine = (lax.axis_size(axis), lax.axis_index(axis))
    everything = jax.tree.map(
        lambda part, kind: lax.all_gather(part.astype(kind), axis), x, (jnp.bfloat16, jnp.bfloat16)
    )
    start = jax.tree.map(
        lambda part, zero: jnp.broadcast_to(jnp.asarray(zero, part.dtype), part.shape), x, identity
    )

    def lap(k, before):
        reached = k < mine
        new = combine(
            before, jax.tree.map(lambda part, own: part[k].astype(own.dtype), everything, x)
        )
        return jax.tree.map(lambda a, b: jnp.where(reached, a, b), new, before)

    return lax.fori_loop(0, size, lap, start)


def convolve(gated, kernel):
    return lax.conv_general_dilated(
        gated[None],
        kernel[:, None, :],
        (1,),
        "VALID",
        dimension_numbers=("NWC", "WIO", "NWC"),
        feature_group_count=gated.shape[1],
        precision=highest_precision,
    )[0]


def channel_norm(values, first_sum, second_sum, gain, bias):
    mean_value = first_sum[:, None] / CONV_CH
    variance = second_sum[:, None] / CONV_CH - mean_value * mean_value
    shifted = (values - mean_value) * lax.rsqrt(variance + layer_eps) * gain + bias
    return jax.nn.silu(shifted).astype(jnp.bfloat16)


def gate_factors(query_projected, forget_projected, forget_floor_margin, decay_jump_rows):
    row_total_count = query_projected.shape[0]
    head_total_count = decay_jump_rows.shape[1]
    query_rows = jax.nn.silu(query_projected.astype(jnp.float32))
    log_forget_gate = jnp.logaddexp(
        jnp.log1p(-forget_floor_margin),
        jnp.log(forget_floor_margin) + jax.nn.log_sigmoid(forget_projected.astype(jnp.float32)),
    )
    key_gate_values = -jnp.expm1(log_forget_gate)
    log_decay_running = (
        log_forget_gate.reshape(row_total_count, head_total_count, -1) + decay_jump_rows[:, :, None]
    )
    return (
        query_rows.reshape(row_total_count, head_total_count, -1),
        key_gate_values.reshape(row_total_count, head_total_count, -1),
        log_decay_running,
    )


def finish(recurrent, gain, outgate_proj):
    row_total_count = recurrent.shape[0]
    scaled = recurrent * lax.rsqrt(
        jnp.mean(recurrent * recurrent, axis=2, keepdims=True) + norm_eps
    )
    gated_out = (
        scaled.reshape(row_total_count, -1) * gain * jax.nn.silu(outgate_proj.astype(jnp.float32))
    )
    return gated_out.astype(jnp.bfloat16)


def combine_states(first_part, second_part):
    return (
        first_part[0] + second_part[0],
        jnp.exp(second_part[0])[:, :, None] * first_part[1] + second_part[1],
    )


def carry_step(recurrence_state, block_parts):
    decay_end, contribution = block_parts
    return (jnp.exp(decay_end)[:, :, None] * recurrence_state + contribution, recurrence_state)


def per_device(
    tokens,
    input_norm_gain,
    convolution_value_weight,
    convolution_gate_weight,
    depthwise_filter_taps,
    channel_norm_gain,
    channel_norm_bias,
    query_projection_weight,
    forget_gate_weight,
    recurrence_value_weight,
    output_gate_weight,
    forget_floor_margin,
    decay_jump_terms,
    head_norm_gain,
    convolution_output_weight,
    recurrence_output_weight,
):
    features = tokens.astype(jnp.float32)
    normed = (
        features
        * lax.rsqrt(jnp.mean(features * features, axis=1, keepdims=True) + norm_eps)
        * input_norm_gain
    ).astype(jnp.bfloat16)
    gathered = (
        lax.all_gather(convolution_value_weight, "sp", axis=0, tiled=True),
        lax.all_gather(convolution_gate_weight, "sp", axis=0, tiled=True),
        lax.all_gather(query_projection_weight, "sp", axis=0, tiled=True),
        lax.all_gather(forget_gate_weight, "sp", axis=0, tiled=True),
        lax.all_gather(recurrence_value_weight, "sp", axis=0, tiled=True),
        lax.all_gather(output_gate_weight, "sp", axis=0, tiled=True),
        lax.all_gather(convolution_output_weight, "sp", axis=1, tiled=True),
        lax.all_gather(recurrence_output_weight, "sp", axis=1, tiled=True),
    )
    projection_weights = gathered[:6]
    conv_columns = gathered[6]
    rec_columns = gathered[7]

    def project(row_piece):
        return jnp.concatenate(
            [
                jnp.dot(row_piece, weight, preferred_element_type=jnp.float32).astype(jnp.bfloat16)
                for weight in projection_weights
            ],
            axis=1,
        )

    projected = project(lax.all_gather(normed, "tp", axis=0, tiled=True))
    offsets = []
    position = 0
    for weight in projection_weights[:-1]:
        position = position + weight.shape[1]
        offsets.append(position)
    value_proj, gate_proj, query_projected, forget_projected, input_proj, outgate_proj = jnp.split(
        projected, offsets, axis=1
    )
    row_total_count = value_proj.shape[0]
    rim_rows = depthwise_filter_taps.shape[0] - 1
    tail_value, tail_gate = passed_along(
        (value_proj[row_total_count - rim_rows :], gate_proj[row_total_count - rim_rows :]), "sp", 1
    )
    value_ext = jnp.concatenate([tail_value, value_proj], axis=0)
    gate_ext = jnp.concatenate([tail_gate, gate_proj], axis=0)
    gated = value_ext.astype(jnp.float32) * jax.nn.sigmoid(gate_ext.astype(jnp.float32))
    convolved = convolve(gated, depthwise_filter_taps).astype(jnp.bfloat16)
    device_heads = decay_jump_terms.shape[0]
    query_rows, key_gate_values, log_decay_running = gate_factors(
        query_projected, forget_projected, forget_floor_margin, decay_jump_terms.T
    )
    input_rows = input_proj.astype(jnp.float32).reshape(row_total_count, device_heads, -1)
    block_count = row_total_count // HG_BLOCK

    def to_blocks(array):
        return array.reshape(block_count, HG_BLOCK, device_heads, -1).transpose(0, 2, 1, 3)

    block_queries = to_blocks(query_rows)
    block_keys = to_blocks(key_gate_values)
    block_inputs = to_blocks(input_rows)
    cumulative = jnp.cumsum(to_blocks(log_decay_running), axis=2)
    final_decay = cumulative[:, :, -1, :]
    query_rows_scaled = block_queries * jnp.exp(cumulative)
    scaled_keys = block_keys * jnp.exp(-cumulative)
    final_keys = block_keys * jnp.exp(final_decay[:, :, None, :] - cumulative)
    attention_scores = jnp.einsum(
        "nhtk,nhsk->nhts", query_rows_scaled, scaled_keys, precision=highest_precision
    )
    causal = jnp.arange(HG_BLOCK)[:, None] >= jnp.arange(HG_BLOCK)[None, :]
    attention_scores = jnp.where(causal[None, None], attention_scores, 0.0)
    inner = jnp.einsum(
        "nhts,nhsv->nhtv", attention_scores, block_inputs, precision=highest_precision
    )
    contributions = jnp.einsum(
        "nhsk,nhsv->nhkv", final_keys, block_inputs, precision=highest_precision
    )
    initial = jnp.zeros((device_heads, HG_DK, HG_DV), jnp.float32)
    local_state, block_starts = lax.scan(carry_step, initial, (final_decay, contributions))
    device_decay = jnp.sum(final_decay, axis=0)
    before_blocks = jnp.cumsum(final_decay, axis=0) - final_decay
    incoming = prefix(
        (device_decay, local_state),
        "sp",
        combine_states,
        (jnp.zeros_like(device_decay), jnp.zeros_like(local_state)),
    )
    starts = block_starts + jnp.exp(before_blocks)[:, :, :, None] * incoming[1][None]
    recurrent = inner + jnp.einsum(
        "nhtk,nhkv->nhtv", query_rows_scaled, starts, precision=highest_precision
    )
    recurrent = recurrent.transpose(0, 2, 1, 3).reshape(row_total_count, device_heads, -1)
    rec_out = finish(recurrent, head_norm_gain, outgate_proj)
    values = convolved.astype(jnp.float32)
    totals = lax.psum((jnp.sum(values, axis=1), jnp.sum(values * values, axis=1)), "tp")
    conv_out = channel_norm(values, totals[0], totals[1], channel_norm_gain, channel_norm_bias)
    conv_part = lax.slice_in_dim(
        conv_out, 0, row_total_count // lax.axis_size("tp") * lax.axis_size("tp"), axis=0
    )
    return lax.psum_scatter(
        (
            jnp.dot(conv_part, conv_columns, preferred_element_type=jnp.float32)
            + jnp.dot(rec_out, rec_columns, preferred_element_type=jnp.float32)
        ).astype(jnp.bfloat16),
        "tp",
        scatter_dimension=0,
        tiled=True,
    )


def solution(mesh):
    in_specs = (
        P(("sp", "tp"), None),
        P(),
        P("sp", "tp"),
        P("sp", "tp"),
        P(None, "tp"),
        P("tp"),
        P("tp"),
        P("sp", "tp"),
        P("sp", "tp"),
        P("sp", "tp"),
        P("sp", "tp"),
        P("tp"),
        P("tp", "sp"),
        P("tp"),
        P("tp", "sp"),
        P("tp", "sp"),
    )
    out_specs = P(("sp", "tp"), None)
    return jax.shard_map(
        per_device, mesh=mesh, in_specs=in_specs, out_specs=out_specs, check_vma=False
    )
```

profile of v0, /device:TPU:0, one launch (start us, length us, event | category | flops | bytes accessed | tf_op | source)
XLA Modules:
  0.0 371.7 jit_solution(17329059093912126885)
XLA Ops:
  6.5 0.7 all-gather.20.cloned.1.call-update
  7.3 0.7 all-gather.22.cloned.1.call-update
  8.1 0.7 all-gather.18.cloned.1.call-update
  8.8 0.5 all-gather.12.cloned.1.call-update
  9.4 0.5 all-gather.14.cloned.1.call-update
  10.0 0.5 all-gather.16.cloned.1.call-update
  10.5 0.7 all-gather.24.cloned.1.call-update
  11.3 0.7 all-gather.26.cloned.1.call-update
  12.1 0.1 fusion.9
  12.3 0.5 copy-done.2
  12.9 8.7 %all_gather.37 = bf16[128,2048]{1,0:T(8,128)(2,1)S(1)} all-gather(bf16[32,2048]{1,0:T(8,128)(2,1)S(1)} %fusion.11), channel_id=1, replica_groups=mesh['sp'=8,'tp'=4] {'tp'}, dimensions={0}, use_global_device_ids=true | all-gather | bytes 655360 | tf_op jit(solution)/shard_map/all_gather | solution.py:148
  21.6 0.7 copy-done.7
  22.4 30.1 %all-gather.20.cloned.1.call-done = bf16[2048,256]{1,0:T(8,128)(2,1)} async-done(((bf16[256,256]{1,0:T(8,128)(2,1)}), bf16[2048,256]{1,0:T(8,128)(2,1)}) %all-gather.20.cloned.1.call-update) | async-done | bytes 1048592 | tf_op jit(solution)/shard_map/all_gather | solution.py:129
  52.5 1.7 exponential-minus-one_negate_fusion
  54.4 0.1 reduce_window_sum.22
  54.6 39.0 %all-gather.22.cloned.1.call-done = bf16[2048,256]{1,0:T(8,128)(2,1)} async-done(((bf16[256,256]{1,0:T(8,128)(2,1)}), bf16[2048,256]{1,0:T(8,128)(2,1)}) %all-gather.22.cloned.1.call-update) | async-done | bytes 1048592 | tf_op jit(solution)/shard_map/all_gather | solution.py:130
  93.6 1.5 convolution_convert_fusion.2
  95.2 0.4 fusion.24
  95.6 0.4 while.27
  96.0 32.5 %all-gather.1 = bf16[16,128,128]{2,1,0:T(8,128)(2,1)S(1)} all-gather(bf16[2,128,128]{2,1,0:T(8,128)(2,1)S(1)} %convert_element_type.128), channel_id=3, replica_groups=mesh['sp'=8,'tp'=4] {'sp'}, dimensions={0}, use_global_device_ids=true | all-gather | bytes 589824 | tf_op jit(solution)/shard_map/all_gather | solution.py:24
  128.5 17.8 %all-gather.2 = bf16[8,2,128]{2,1,0:T(2,128)(2,1)S(1)} all-gather(bf16[1,2,128]{2,1,0:T(2,128)(2,1)S(1)} %bitcast.113), channel_id=2, replica_groups=mesh['sp'=8,'tp'=4] {'sp'}, dimensions={0}, use_global_device_ids=true | all-gather | bytes 4608 | tf_op jit(solution)/shard_map/all_gather | solution.py:24
  146.3 1.4 while.28
  146.3 0.1 fusion.69
  146.5 0.1 fusion.69
  146.7 0.1 fusion.69
  146.9 0.1 fusion.69
  147.2 0.1 fusion.69
  147.7 1.6 divide_multiply_fusion.1
  149.4 28.2 %all-gather.12.cloned.1.call-done = bf16[2048,256]{1,0:T(8,128)(2,1)} async-done(((bf16[256,256]{1,0:T(8,128)(2,1)}), bf16[2048,256]{1,0:T(8,128)(2,1)}) %all-gather.12.cloned.1.call-update) | async-done | bytes 1048592 | tf_op jit(solution)/shard_map/all_gather | solution.py:126
  177.6 1.5 convolution_convert_fusion.6
  179.1 2.5 collective-permute-start
  181.6 36.9 %all-gather.14.cloned.1.call-done = bf16[2048,256]{1,0:T(8,128)(2,1)} async-done(((bf16[256,256]{1,0:T(8,128)(2,1)}), bf16[2048,256]{1,0:T(8,128)(2,1)}) %all-gather.14.cloned.1.call-update) | async-done | bytes 1048592 | tf_op jit(solution)/shard_map/all_gather | solution.py:127
  218.6 1.5 convolution_convert_fusion.5
  220.1 2.5 collective-permute-start.1
  222.6 0.4 convolution_select_fusion
  223.0 0.2 fusion.36
  223.2 0.5 multiply_reduce_fusion
  224.2 2.2 fusion.51
  226.4 5.7 %all-reduce = (f32[128]{0:T(128)S(1)}, f32[128]{0:T(128)S(1)}) all-reduce(f32[128]{0:T(128)S(1)} %fusion.23, f32[128]{0:T(128)S(1)} %get-tuple-element.194), channel_id=1, replica_groups=mesh['sp'=8,'tp'=4] {'tp'}, use_global_device_ids=true, to_apply=%region_4.5 | all-reduce | flops 256 | bytes 2048 | tf_op jit(solution)/shard_map/psum | solution.py:212
  232.1 26.5 %all-gather.16.cloned.1.call-done = bf16[256,2048]{1,0:T(8,128)(2,1)} async-done(((bf16[256,256]{1,0:T(8,128)(2,1)}), bf16[256,2048]{1,0:T(8,128)(2,1)}) %all-gather.16.cloned.1.call-update) | async-done | bytes 1048592 | tf_op jit(solution)/shard_map/all_gather | solution.py:132
  258.7 0.7 copy-done.3
  259.3 1.6 fusion.34
  261.0 39.2 %all-gather.24.cloned.1.call-done = bf16[2048,256]{1,0:T(8,128)(2,1)} async-done(((bf16[256,256]{1,0:T(8,128)(2,1)}), bf16[2048,256]{1,0:T(8,128)(2,1)}) %all-gather.24.cloned.1.call-update) | async-done | bytes 1048592 | tf_op jit(solution)/shard_map/all_gather | solution.py:131
  300.1 40.2 %all-gather.26.cloned.1.call-done = bf16[256,2048]{1,0:T(8,128)(2,1)} async-done(((bf16[256,256]{1,0:T(8,128)(2,1)}), bf16[256,2048]{1,0:T(8,128)(2,1)}) %all-gather.26.cloned.1.call-update) | async-done | bytes 1048592 | tf_op jit(solution)/shard_map/all_gather | solution.py:133
  340.3 0.2 mul.161
  340.5 0.7 copy-done.5
  341.2 3.1 fusion.1
  344.3 20.9 %reduce-scatter.2.cloned.1.call-done = bf16[32,2048]{1,0:T(8,128)(2,1)} async-done(((bf16[128,2048]{1,0:T(8,128)(2,1)}), bf16[32,2048]{1,0:T(8,128)(2,1)}) %reduce-scatter.2.cloned.1.call-update) | async-done | bytes 131088 | tf_op jit(solution)/shard_map/reduce_scatter | solution.py:217
  (67 shorter events, 2.2 us)
Async XLA Ops:
  6.5 217.6 %copy-start = (f32[31,256]{1,0:T(8,128)S(1)}, f32[31,256]{1,0:T(8,128)}, u32[]{:S(2)}) copy-start(f32[31,256]{1,0:T(8,128)} %param.24) | copy-start | bytes 95236
  6.5 46.0 %all-gather.20.cloned.1.call-start = ((), (), s32[]{:S(2)}) async-start(), calls=%async_computation.5 | async-start | bytes 1179648 | tf_op jit(solution)/shard_map/all_gather | solution.py:129
  7.3 86.4 %all-gather.22.cloned.1.call-start = ((), (), s32[]{:S(2)}) async-start(), calls=%async_computation.6 | async-start | bytes 1179648 | tf_op jit(solution)/shard_map/all_gather | solution.py:130
  8.0 139.7 %all-gather.18.cloned.1.call-start = ((), (), s32[]{:S(2)}) async-start(), calls=%async_computation.4 | async-start | bytes 1179648 | tf_op jit(solution)/shard_map/all_gather | solution.py:128
  8.7 168.8 %all-gather.12.cloned.1.call-start = ((), (), s32[]{:S(2)}) async-start(), calls=%async_computation.1 | async-start | bytes 1179648 | tf_op jit(solution)/shard_map/all_gather | solution.py:126
  9.3 209.3 %all-gather.14.cloned.1.call-start = ((), (), s32[]{:S(2)}) async-start(), calls=%async_computation.2 | async-start | bytes 1179648 | tf_op jit(solution)/shard_map/all_gather | solution.py:127
  9.9 248.8 %all-gather.16.cloned.1.call-start = ((), (), s32[]{:S(2)}) async-start(), calls=%async_computation.3 | async-start | bytes 1179648 | tf_op jit(solution)/shard_map/all_gather | solution.py:132
  10.5 1.6 copy-start.1
  10.5 289.6 %all-gather.24.cloned.1.call-start = ((), (), s32[]{:S(2)}) async-start(), calls=%async_computation.7 | async-start | bytes 1179648 | tf_op jit(solution)/shard_map/all_gather | solution.py:131
  11.2 329.1 %all-gather.26.cloned.1.call-start = ((), (), s32[]{:S(2)}) async-start(), calls=%async_computation.8 | async-start | bytes 1179648 | tf_op jit(solution)/shard_map/all_gather | solution.py:133
  12.0 353.2 %reduce-scatter.2.cloned.1.call-start = ((), (), s32[]{:S(2)}) async-start(), calls=%async_computation.9 | async-start | bytes 655360 | tf_op jit(solution)/shard_map/reduce_scatter | solution.py:217
  12.1 0.7 copy-start.2
  12.9 8.7 %copy-start.6 = (f32[256]{0:T(256)S(1)}, f32[256]{0:T(256)}, u32[]{:S(2)}) copy-start(f32[256]{0:T(256)} %param.31) | copy-start | bytes 3076
  21.6 0.7 copy-start.7
  179.1 44.9 %collective-permute-start = (bf16[30,256]{1,0:T(8,128)(2,1)S(1)}, bf16[30,256]{1,0:T(8,128)(2,1)S(1)}, u32[]{:S(2)}, u32[]{:S(2)}) collective-permute-start(bf16[30,256]{1,0:T(8,128)(2,1)S(1)} %slice.12), channel_id=1, source_target_pairs={{0,4},{4,8},{8,12},{12,16},{16,20},{20,24},{24,28},{1,5},{5,9},{9,... | collective-permute-start | bytes 46088 | tf_op jit(solution)/shard_map/ppermute | solution.py:18
  220.1 3.9 %collective-permute-start.1 = (bf16[30,256]{1,0:T(8,128)(2,1)S(1)}, bf16[30,256]{1,0:T(8,128)(2,1)S(1)}, u32[]{:S(2)}, u32[]{:S(2)}) collective-permute-start(bf16[30,256]{1,0:T(8,128)(2,1)S(1)} %slice.13), channel_id=1, source_target_pairs={{0,4},{4,8},{8,12},{12,16},{16,20},{20,24},{24,28},{1,5},{5,9},{9,... | collective-permute-start | bytes 46088 | tf_op jit(solution)/shard_map/ppermute | solution.py:18
  224.1 34.5 %copy-start.4 = (f32[256]{0:T(256)S(1)}, f32[256]{0:T(256)}, u32[]{:S(2)}) copy-start(f32[256]{0:T(256)} %param.25) | copy-start | bytes 3076
  258.7 0.7 copy-start.3
  340.5 0.7 copy-start.5
Sparse Core Ops, SparseCore 0:
  9.5 42.9 all-gather.19
  54.6 38.9 all-gather.21
  95.8 40.5 all-gather.17
  138.4 39.1 all-gather.11
  179.6 38.9 all-gather.13
  220.5 38.1 all-gather.15
  260.8 39.2 all-gather.23
  302.2 38.0 all-gather.25
  344.5 20.6 reduce-scatter.1
where the time goes:
time: 372 us
  waiting for transfers between devices  266 us (72%)
  blocking collectives  64.7 us (17%)
  matrix products  16.3 us (4%)
  between operations  13.5 us (4%)
  starting transfers between devices  5.28 us (1%)
    all_gather x2, blocking collectives, prefix(): lax.all_gather(part.astype(kind), axis)  50.3 us
    all_gather x1, waiting for transfers between devices, per_device(): lax.all_gather(recurrence_output_weight, 'sp', axis=1, tiled=True)  40.2 us
    all_gather x1, waiting for transfers between devices, per_device(): lax.all_gather(output_gate_weight, 'sp', axis=0, tiled=True)  39.2 us
    all_gather x1, waiting for transfers between devices, per_device(): lax.all_gather(recurrence_value_weight, 'sp', axis=0, tiled=True)  39 us
    all_gather x1, waiting for transfers between devices, per_device(): lax.all_gather(convolution_gate_weight, 'sp', axis=0, tiled=True)  36.9 us
    all_gather x1, waiting for transfers between devices, per_device(): lax.all_gather(forget_gate_weight, 'sp', axis=0, tiled=True)  30.1 us
    all_gather x1, waiting for transfers between devices, per_device(): lax.all_gather(convolution_value_weight, 'sp', axis=0, tiled=True)  28.2 us
    all_gather x1, waiting for transfers between devices, per_device(): lax.all_gather(convolution_output_weight, 'sp', axis=1, tiled=True)  26.5 us
  transfers between devices with their start and end apart: 11, of which 8 were waited for; matrix products, arithmetic and copies ran while one was open for 4% of the time, Pallas kernels for 0%

commit v1 on v0

--- a/solution.py
+++ b/solution.py
@@ -124,7 +124,10 @@
     ).astype(jnp.bfloat16)
     gathered = (
         lax.all_gather(convolution_value_weight, "sp", axis=0, tiled=True),
-        lax.all_gather(convolution_gate_weight, "sp", axis=0, tiled=True),
+        jnp.concatenate(
+            lax.all_to_all(jnp.stack([convolution_gate_weight] * lax.axis_size("sp")), "sp", 0, 0),
+            axis=0,
+        ),
         lax.all_gather(query_projection_weight, "sp", axis=0, tiled=True),
         lax.all_gather(forget_gate_weight, "sp", axis=0, tiled=True),
         lax.all_gather(recurrence_value_weight, "sp", axis=0, tiled=True),

time: 372 us -> 339 us (0.911)
  waiting for transfers between devices: 266 us -> 227 us
  starting transfers between devices: 5.28 us -> 12.6 us
    all_gather x1 -> x0, waiting for transfers between devices: 36.9 us -> none  [per_device(): lax.all_gather(convolution_gate_weight, 'sp', axis=0, tiled=True)]
    all_to_all x0 -> x1, starting transfers between devices: none -> 7.28 us  [per_device(): lax.all_to_all(jnp.stack([convolution_gate_weight] * lax.axis_size('sp'))...]
  transfers between devices with their start and end apart: 11 -> 11, of which waited for: 8 -> 8; matrix products, arithmetic and copies ran while one was open for 4% -> 5% of each run, Pallas kernels for 0% -> 0%
where the time goes in v1:
time: 339 us
  waiting for transfers between devices  227 us (67%)
  blocking collectives  63.1 us (19%)
  matrix products  15.1 us (4%)
  between operations  13.8 us (4%)
  starting transfers between devices  12.6 us (4%)
  local copies, waits for them, and re-layouts  4.45 us (1%)
    all_gather x2, blocking collectives, prefix(): lax.all_gather(part.astype(kind), axis)  50.2 us
    all_gather x1, waiting for transfers between devices, per_device(): lax.all_gather(recurrence_output_weight, 'sp', axis=1, tiled=True)  40.2 us
    all_gather x1, waiting for transfers between devices, per_device(): lax.all_gather(recurrence_value_weight, 'sp', axis=0, tiled=True)  39.1 us
    all_gather x1, waiting for transfers between devices, per_device(): lax.all_gather(output_gate_weight, 'sp', axis=0, tiled=True)  39 us
    all_gather x1, waiting for transfers between devices, per_device(): lax.all_gather(forget_gate_weight, 'sp', axis=0, tiled=True)  31.8 us
    all_gather x1, waiting for transfers between devices, per_device(): lax.all_gather(convolution_output_weight, 'sp', axis=1, tiled=True)  26.5 us
    all_gather x1, waiting for transfers between devices, per_device(): lax.all_gather(convolution_value_weight, 'sp', axis=0, tiled=True)  25.5 us
    reduce_scatter x1, waiting for transfers between devices, per_device(): lax.psum_scatter((jnp.dot(conv_part, conv_columns, preferred_element_type...  20.9 us
  transfers between devices with their start and end apart: 11, of which 8 were waited for; matrix products, arithmetic and copies ran while one was open for 5% of the time, Pallas kernels for 0%

profile of v1, /device:TPU:0, one launch (start us, length us, event | category | flops | bytes accessed | tf_op | source)
XLA Modules:
  0.0 338.8 jit_solution(12769308794320723816)
XLA Ops:
  6.5 0.7 all-gather.17.cloned.1.call-update
  7.3 0.7 all-gather.19.cloned.1.call-update
  8.1 0.7 all-gather.15.cloned.1.call-update
  8.8 0.5 all-gather.11.cloned.1.call-update
  9.4 0.5 all-gather.13.cloned.1.call-update
  10.0 0.5 all-gather.21.cloned.1.call-update
  10.5 1.0 stack.2
  11.5 7.3 %all-to-all-start = ((bf16[8,256,256]{2,1,0:T(8,128)(2,1)}), bf16[8,256,256]{2,1,0:T(8,128)(2,1)S(1)}, u32[]{:S(2)}, u32[]{:S(2)}) async-start(bf16[8,256,256]{2,1,0:T(8,128)(2,1)} %stack.2), calls=%async_computation | async-start | bytes 2097152 | tf_op jit(solution)/shard_map/all_to_all | solution.py:128
  18.9 0.7 all-gather.23.cloned.1.call-update
  19.7 0.1 fusion.9
  19.9 0.5 copy-done.3
  20.5 7.2 %all_gather.34 = bf16[128,2048]{1,0:T(8,128)(2,1)S(1)} all-gather(bf16[32,2048]{1,0:T(8,128)(2,1)S(1)} %fusion.11), channel_id=1, replica_groups=mesh['sp'=8,'tp'=4] {'tp'}, dimensions={0}, use_global_device_ids=true | all-gather | bytes 655360 | tf_op jit(solution)/shard_map/all_gather | solution.py:151
  27.8 0.7 copy-done.8
  28.5 31.8 %all-gather.17.cloned.1.call-done = bf16[2048,256]{1,0:T(8,128)(2,1)} async-done(((bf16[256,256]{1,0:T(8,128)(2,1)}), bf16[2048,256]{1,0:T(8,128)(2,1)}) %all-gather.17.cloned.1.call-update) | async-done | bytes 1048592 | tf_op jit(solution)/shard_map/all_gather | solution.py:132
  60.4 1.7 exponential-minus-one_negate_fusion
  62.3 0.1 reduce_window_sum.22
  62.5 39.1 %all-gather.19.cloned.1.call-done = bf16[2048,256]{1,0:T(8,128)(2,1)} async-done(((bf16[256,256]{1,0:T(8,128)(2,1)}), bf16[2048,256]{1,0:T(8,128)(2,1)}) %all-gather.19.cloned.1.call-update) | async-done | bytes 1048592 | tf_op jit(solution)/shard_map/all_gather | solution.py:133
  101.6 1.5 convolution_convert_fusion.2
  103.1 0.4 fusion.24
  103.5 0.4 while.27
  103.9 32.5 %all-gather.1 = bf16[16,128,128]{2,1,0:T(8,128)(2,1)S(1)} all-gather(bf16[2,128,128]{2,1,0:T(8,128)(2,1)S(1)} %convert_element_type.128), channel_id=3, replica_groups=mesh['sp'=8,'tp'=4] {'sp'}, dimensions={0}, use_global_device_ids=true | all-gather | bytes 589824 | tf_op jit(solution)/shard_map/all_gather | solution.py:24
  136.4 17.7 %all-gather.2 = bf16[8,2,128]{2,1,0:T(2,128)(2,1)S(1)} all-gather(bf16[1,2,128]{2,1,0:T(2,128)(2,1)S(1)} %bitcast.115), channel_id=2, replica_groups=mesh['sp'=8,'tp'=4] {'sp'}, dimensions={0}, use_global_device_ids=true | all-gather | bytes 4608 | tf_op jit(solution)/shard_map/all_gather | solution.py:24
  154.1 1.5 divide_multiply_fusion.1
  155.8 1.4 while.28
  155.8 0.1 fusion.69
  156.0 0.1 fusion.69
  156.1 0.1 fusion.69
  156.3 0.1 fusion.69
  156.5 0.1 fusion.69
  157.2 0.3 convolution_convert_fusion.5
  157.5 2.5 collective-permute-start.1
  160.0 25.5 %all-gather.11.cloned.1.call-done = bf16[2048,256]{1,0:T(8,128)(2,1)} async-done(((bf16[256,256]{1,0:T(8,128)(2,1)}), bf16[2048,256]{1,0:T(8,128)(2,1)}) %all-gather.11.cloned.1.call-update) | async-done | bytes 1048592 | tf_op jit(solution)/shard_map/all_gather | solution.py:126
  185.6 1.5 convolution_convert_fusion.6
  187.1 2.5 collective-permute-start
  189.6 0.4 convolution_select_fusion
  190.0 0.2 fusion.36
  190.2 0.5 multiply_reduce_fusion
  191.1 2.2 fusion.51
  193.4 5.7 %all-reduce = (f32[128]{0:T(128)S(1)}, f32[128]{0:T(128)S(1)}) all-reduce(f32[128]{0:T(128)S(1)} %fusion.23, f32[128]{0:T(128)S(1)} %get-tuple-element.194), channel_id=1, replica_groups=mesh['sp'=8,'tp'=4] {'tp'}, use_global_device_ids=true, to_apply=%region_4.5 | all-reduce | flops 256 | bytes 2048 | tf_op jit(solution)/shard_map/psum | solution.py:215
  199.1 26.5 %all-gather.13.cloned.1.call-done = bf16[256,2048]{1,0:T(8,128)(2,1)} async-done(((bf16[256,256]{1,0:T(8,128)(2,1)}), bf16[256,2048]{1,0:T(8,128)(2,1)}) %all-gather.13.cloned.1.call-update) | async-done | bytes 1048592 | tf_op jit(solution)/shard_map/all_gather | solution.py:135
  225.6 0.7 copy-done.4
  226.3 1.6 fusion.34
  227.9 39.0 %all-gather.21.cloned.1.call-done = bf16[2048,256]{1,0:T(8,128)(2,1)} async-done(((bf16[256,256]{1,0:T(8,128)(2,1)}), bf16[2048,256]{1,0:T(8,128)(2,1)}) %all-gather.21.cloned.1.call-update) | async-done | bytes 1048592 | tf_op jit(solution)/shard_map/all_gather | solution.py:134
  266.9 40.2 %all-gather.23.cloned.1.call-done = bf16[256,2048]{1,0:T(8,128)(2,1)} async-done(((bf16[256,256]{1,0:T(8,128)(2,1)}), bf16[256,2048]{1,0:T(8,128)(2,1)}) %all-gather.23.cloned.1.call-update) | async-done | bytes 1048592 | tf_op jit(solution)/shard_map/all_gather | solution.py:136
  307.1 0.2 mul.161
  307.3 0.7 copy-done.6
  308.0 3.2 fusion.1
  311.1 20.9 %reduce-scatter.2.cloned.1.call-done = bf16[32,2048]{1,0:T(8,128)(2,1)} async-done(((bf16[128,2048]{1,0:T(8,128)(2,1)}), bf16[32,2048]{1,0:T(8,128)(2,1)}) %reduce-scatter.2.cloned.1.call-update) | async-done | bytes 131088 | tf_op jit(solution)/shard_map/reduce_scatter | solution.py:220
  (69 shorter events, 2.2 us)
Async XLA Ops:
  6.5 184.6 %copy-start = (f32[31,256]{1,0:T(8,128)S(1)}, f32[31,256]{1,0:T(8,128)}, u32[]{:S(2)}) copy-start(f32[31,256]{1,0:T(8,128)} %param.24) | copy-start | bytes 95236
  6.5 53.8 %all-gather.17.cloned.1.call-start = ((), (), s32[]{:S(2)}) async-start(), calls=%async_computation.5 | async-start | bytes 1179648 | tf_op jit(solution)/shard_map/all_gather | solution.py:132
  7.3 94.3 %all-gather.19.cloned.1.call-start = ((), (), s32[]{:S(2)}) async-start(), calls=%async_computation.6 | async-start | bytes 1179648 | tf_op jit(solution)/shard_map/all_gather | solution.py:133
  8.0 146.1 %all-gather.15.cloned.1.call-start = ((), (), s32[]{:S(2)}) async-start(), calls=%async_computation.4 | async-start | bytes 1179648 | tf_op jit(solution)/shard_map/all_gather | solution.py:131
  8.7 176.8 %all-gather.11.cloned.1.call-start = ((), (), s32[]{:S(2)}) async-start(), calls=%async_computation.2 | async-start | bytes 1179648 | tf_op jit(solution)/shard_map/all_gather | solution.py:126
  9.3 1.2 copy-start.2
  9.3 216.3 %all-gather.13.cloned.1.call-start = ((), (), s32[]{:S(2)}) async-start(), calls=%async_computation.3 | async-start | bytes 1179648 | tf_op jit(solution)/shard_map/all_gather | solution.py:135
  9.9 257.0 %all-gather.21.cloned.1.call-start = ((), (), s32[]{:S(2)}) async-start(), calls=%async_computation.7 | async-start | bytes 1179648 | tf_op jit(solution)/shard_map/all_gather | solution.py:134
  11.5 145.6 %all-to-all-start = ((bf16[8,256,256]{2,1,0:T(8,128)(2,1)}), bf16[8,256,256]{2,1,0:T(8,128)(2,1)S(1)}, u32[]{:S(2)}, u32[]{:S(2)}) async-start(bf16[8,256,256]{2,1,0:T(8,128)(2,1)} %stack.2), calls=%async_computation | async-start | bytes 2097152 | tf_op jit(solution)/shard_map/all_to_all | solution.py:128
  18.8 0.9 copy-start.1
  18.8 288.3 %all-gather.23.cloned.1.call-start = ((), (), s32[]{:S(2)}) async-start(), calls=%async_computation.8 | async-start | bytes 1179648 | tf_op jit(solution)/shard_map/all_gather | solution.py:136
  19.6 312.4 %reduce-scatter.2.cloned.1.call-start = ((), (), s32[]{:S(2)}) async-start(), calls=%async_computation.9 | async-start | bytes 655360 | tf_op jit(solution)/shard_map/reduce_scatter | solution.py:220
  19.7 0.7 copy-start.3
  20.5 7.2 %copy-start.7 = (f32[256]{0:T(256)S(1)}, f32[256]{0:T(256)}, u32[]{:S(2)}) copy-start(f32[256]{0:T(256)} %param.31) | copy-start | bytes 3076
  27.8 0.7 copy-start.8
  157.5 33.5 %collective-permute-start.1 = (bf16[30,256]{1,0:T(8,128)(2,1)S(1)}, bf16[30,256]{1,0:T(8,128)(2,1)S(1)}, u32[]{:S(2)}, u32[]{:S(2)}) collective-permute-start(bf16[30,256]{1,0:T(8,128)(2,1)S(1)} %slice.13), channel_id=1, source_target_pairs={{0,4},{4,8},{8,12},{12,16},{16,20},{20,24},{24,28},{1,5},{5,9},{9,... | collective-permute-start | bytes 46088 | tf_op jit(solution)/shard_map/ppermute | solution.py:18
  187.1 3.9 %collective-permute-start = (bf16[30,256]{1,0:T(8,128)(2,1)S(1)}, bf16[30,256]{1,0:T(8,128)(2,1)S(1)}, u32[]{:S(2)}, u32[]{:S(2)}) collective-permute-start(bf16[30,256]{1,0:T(8,128)(2,1)S(1)} %slice.12), channel_id=1, source_target_pairs={{0,4},{4,8},{8,12},{12,16},{16,20},{20,24},{24,28},{1,5},{5,9},{9,... | collective-permute-start | bytes 46088 | tf_op jit(solution)/shard_map/ppermute | solution.py:18
  191.1 34.5 %copy-start.5 = (f32[256]{0:T(256)S(1)}, f32[256]{0:T(256)}, u32[]{:S(2)}) copy-start(f32[256]{0:T(256)} %param.25) | copy-start | bytes 3076
  225.6 0.7 copy-start.4
  307.3 0.7 copy-start.6
Sparse Core Ops, SparseCore 0:
  9.5 50.8 all-gather.16
  62.5 39.0 all-gather.18
  103.7 40.5 all-gather.14
  146.3 39.2 all-gather.10
  187.5 38.0 all-gather.12
  227.6 39.2 all-gather.20
  268.9 38.0 all-gather.22
  311.3 20.6 reduce-scatter.1
